TPU v7x, 256 devices: a whole 4x4x8 slice. The times are simulated.
256 devices in a mesh: sp: 32 (over z, x), tp: 8 (over y, core).
Axes of the slice: x: 4, y: 4, z: 8, core: 2. Of those that a mesh axis runs over, the one named last changes fastest.
Arguments:
- tokens: bfloat16 [16384, 2048], P(('sp', 'tp')), may hold values from -6 to 6
- norm_gain: float32 [2048], replicated, may hold values from 0.1 to 1.9
- rec_query: bfloat16 [2048, 1024], P(None, 'tp'), may hold values from -0.125 to 0.125
- fwd_gate: bfloat16 [2048, 1024], P(None, 'tp'), may hold values from -0.125 to 0.125
- bwd_gate: bfloat16 [2048, 1024], P(None, 'tp'), may hold values from -0.125 to 0.125
- rec_value: bfloat16 [2048, 1024], P(None, 'tp'), may hold values from -0.125 to 0.125
- gate_leak: float32 [2, 1024], P(None, 'tp'), may hold values from 0 to 0.08, as said below
- log_decay: float32 [2, 16384, 8], P(None, 'sp', 'tp'), may hold values from -2.2 to 0, as said below
- rec_gain: float32 [128], replicated, may hold values from 0.1 to 1.9
- att_query: bfloat16 [2048, 1024], P(None, 'tp'), as said below
- att_key: bfloat16 [2048, 1024], P(None, 'tp')
- att_value: bfloat16 [2048, 1024], P(None, 'tp'), may hold values from -0.125 to 0.125
- lambdas: float32 [8], P('tp'), may hold values from 0.3 to 0.8
- att_gain: float32 [128], replicated, may hold values from 0.1 to 1.9
- out_rec: bfloat16 [1024, 2048], replicated, may hold values from -0.125 to 0.125
- out_att: bfloat16 [1024, 2048], replicated, may hold values from -0.125 to 0.125
Outputs:
- layer_out: bfloat16 [16384, 2048], P(('sp', 'tp'))
Inputs may be any that keep to these rules, and one draw needn't show every extreme that they name: `gate_leak`: positive, by direction and channel. `log_decay`: never positive. `att_query`: entries of order 2048 to the power -1/2.
All inputs are finite; a program needn't handle non-finite values.
Results may differ from a plain program's by a relative error of at most 0.011.
Values may be sent and summed in bfloat16 or wider, within the bound.
A program may use at most 128 MiB of HBM per device.

v0:
```python
import math

import jax
import jax.numpy as jnp
from jax import lax
from jax.sharding import Mesh
from jax.sharding import PartitionSpec as P

HK = 128
HV = 128
AK = 64
AV = 128
BLOCK = 64
SP = ("sp_0", "sp_1")
SP_TP = ("sp_0", "sp_1", "tp")


EPS = 1e-06
THETA = 500000.0


def joined_along(pieces, dim):
    dims = list(pieces.shape[1:])
    dims[dim] *= pieces.shape[0]
    return jnp.moveaxis(pieces, 0, dim).reshape(dims)


def copy_for_each(value, axis):
    copies = jnp.broadcast_to(value, (lax.axis_size(axis), *value.shape))
    return lax.all_to_all(copies, axis, split_axis=0, concat_axis=0, tiled=True)


def gathered_copies(value, axis, dim):
    return joined_along(copy_for_each(value, axis), dim)


def nothing_yet(value, identity):
    return jax.tree.map(
        lambda part, zero: jnp.zeros_like(part) + jnp.asarray(zero, part.dtype), value, identity
    )


def all_in_one(value, axis):
    leaves = jax.tree.leaves(value)
    order = sorted(range(len(leaves)), key=lambda k: -leaves[k].size)
    width = (1, *leaves[order[0]].shape)[-1]
    lines = [
        jnp.pad(leaves[k].reshape(-1), (0, -leaves[k].size % width)).reshape(-1, width)
        for k in order
    ]
    both, at, found = (lax.all_gather(jnp.concatenate(lines), axis), 0, {})
    for k, line in zip(order, lines):
        piece = both[:, at : at + len(line)].reshape(len(both), -1)
        found[k] = piece[:, : leaves[k].size].reshape(-1, *leaves[k].shape)
        at += len(line)
    numbers = iter(range(len(leaves)))
    return jax.tree.map(lambda _: found[next(numbers)], value)


def entering(value, axes, combine, identity, reverse):
    before = start = nothing_yet(value, identity)
    subtotal = value
    for axis in reversed(axes):
        size, position = (lax.axis_size(axis), lax.axis_index(axis))
        pieces = all_in_one(
            jax.tree.map(
                lambda part, kind: part.astype(kind), subtotal, (jnp.bfloat16, jnp.bfloat16)
            ),
            axis,
        )
        inside, subtotal = (start, start)
        for k in reversed(range(size)) if reverse else range(size):
            passed = k > position if reverse else k < position
            subtotal = combine(
                subtotal, jax.tree.map(lambda part, own: part[k].astype(own.dtype), pieces, value)
            )
            inside = jax.tree.map(lambda new, old: jnp.where(passed, new, old), subtotal, inside)
        before = combine(inside, before)
    return before


def in_one_piece(arrays, axis, dim, along):
    ends, at = ([], 0)
    for a in arrays[:-1]:
        at += a.shape[along]
        ends.append(at)
    both = jnp.concatenate(arrays, axis=along)
    return tuple(jnp.split(lax.all_gather(both, axis, axis=dim, tiled=True), ends, axis=along))


def rms_scale(values, gain):
    return values * lax.rsqrt(jnp.mean(values * values, axis=-1, keepdims=True) + EPS) * gain


def block_recurrence(queries, keys_in, values, log_forget):
    head_count, length, key_width = queries.shape
    value_width = values.shape[-1]
    block_count = length // BLOCK
    block_shape = (head_count, block_count, BLOCK, key_width)
    query_blocks = queries.reshape(block_shape)
    key_blocks = keys_in.reshape(block_shape)
    value_blocks = values.reshape(head_count, block_count, BLOCK, value_width)
    cumulative = jnp.cumsum(log_forget.reshape(block_shape), axis=2)
    middle = cumulative[:, :, BLOCK // 2 - 1 : BLOCK // 2]
    block_last = cumulative[:, :, BLOCK - 1 :]
    scores = jnp.einsum(
        "hntd,hnsd->hnts",
        query_blocks * jnp.exp(cumulative - middle),
        key_blocks * jnp.exp(middle - cumulative),
    )
    causal_mask = jnp.arange(BLOCK)[:, None] >= jnp.arange(BLOCK)[None, :]
    scores = jnp.where(causal_mask, scores, 0.0)
    within_out = jnp.einsum("hnts,hnsv->hntv", scores, value_blocks)
    per_block_state = jnp.einsum(
        "hnsd,hnsv->hndv", key_blocks * jnp.exp(block_last - cumulative), value_blocks
    )
    block_decay = jnp.exp(block_last[:, :, 0])

    def advance(running, inputs_now):
        factor, added_state = inputs_now
        return (factor[..., None] * running + added_state, running)

    initial = jnp.zeros((head_count, key_width, value_width), jnp.float32)
    end_state, before = lax.scan(
        advance, initial, (jnp.moveaxis(block_decay, 1, 0), jnp.moveaxis(per_block_state, 1, 0))
    )
    before = jnp.moveaxis(before, 0, 1)
    carried = jnp.einsum("hntd,hndv->hntv", query_blocks * jnp.exp(cumulative), before)
    return ((within_out + carried).reshape(head_count, length, value_width), end_state, cumulative)


def local_direction(queries, keys_in, values, log_forget):
    outputs, end_state, cumulative = block_recurrence(queries, keys_in, values, log_forget)
    head_count, length, key_width = queries.shape
    block_totals = cumulative[:, :, BLOCK - 1]
    before_block = jnp.cumsum(block_totals, axis=1) - block_totals
    within = (cumulative + before_block[:, :, None]).reshape(head_count, length, key_width)
    return (outputs, jnp.exp(jnp.sum(block_totals, axis=1)), end_state, queries * jnp.exp(within))


def link(earlier, later):
    return (earlier[0] * later[0], later[0][..., None] * earlier[1] + later[1])


def rotate(vectors, positions):
    half_width = AK // 2
    frequency = THETA ** (-(jnp.arange(half_width, dtype=jnp.float32) * 2.0 / AK))
    angles = positions[:, None] * frequency[None, :]
    cosine = jnp.cos(angles)[:, None, None, :]
    sines = jnp.sin(angles)[:, None, None, :]
    first_half = vectors[..., :half_width]
    second = vectors[..., half_width:]
    return jnp.concatenate(
        [first_half * cosine - second * sines, second * cosine + first_half * sines], axis=-1
    )


def attend(carry, queries, key_rows, value_rows):
    head_count = queries.shape[1]
    row_count = key_rows.shape[0]
    span_rows = math.gcd(row_count, 1024)
    key_blocks = key_rows.reshape(row_count // span_rows, span_rows, head_count, 2, AK)
    value_blocks = value_rows.reshape(row_count // span_rows, span_rows, head_count, AV)

    def absorb(running, inputs_now):
        peak_values, totals, summed = running
        key_block, value_block = inputs_now
        scores = jnp.einsum(
            "qhmd,khmd->hmqk", queries, key_block, preferred_element_type=jnp.float32
        )
        raised = jnp.maximum(peak_values, jnp.max(scores, axis=-1))
        shrink = jnp.exp(peak_values - raised)
        weights_raw = jnp.exp(scores - raised[..., None])
        totals = totals * shrink + jnp.sum(weights_raw, axis=-1)
        summed = summed * shrink[..., None] + jnp.einsum(
            "hmqk,khv->hmqv",
            weights_raw.astype(jnp.bfloat16),
            value_block,
            preferred_element_type=jnp.float32,
        )
        return ((raised, totals, summed), None)

    running, unused = lax.scan(absorb, carry, (key_blocks, value_blocks))
    return running


def on_device(
    tokens,
    norm_gain,
    rec_query,
    fwd_gate,
    bwd_gate,
    rec_value,
    gate_leak,
    log_decay,
    rec_gain,
    att_query,
    att_key,
    att_value,
    lambdas,
    att_gain,
    out_rec,
    out_att,
):
    normed = rms_scale(tokens.astype(jnp.float32), norm_gain).astype(jnp.bfloat16)
    weights_all = (rec_query, fwd_gate, bwd_gate, rec_value, att_query, att_key, att_value)
    joined = jnp.concatenate(weights_all, axis=1)
    projected = jnp.dot(
        gathered_copies(normed, "tp", 0), joined, preferred_element_type=jnp.float32
    ).astype(jnp.bfloat16)
    length = projected.shape[0]
    columns = []
    column_start = 0
    for weight in weights_all:
        columns.append(projected[:, column_start : column_start + weight.shape[1]])
        column_start = column_start + weight.shape[1]
    query_raw, fwd_raw, bwd_raw, value_raw, att_query_raw, att_key_raw, att_value_raw = columns

    def split_heads(table, width):
        return table.astype(jnp.float32).reshape(length, -1, width).transpose(1, 0, 2)

    queries = jax.nn.silu(split_heads(query_raw, HK))
    values = split_heads(value_raw, HV)
    rec_heads = queries.shape[0]
    key_fwd = gate_leak[0].reshape(rec_heads, 1, HK) * jax.nn.sigmoid(-split_heads(fwd_raw, HK))
    key_bwd = gate_leak[1].reshape(rec_heads, 1, HK) * jax.nn.sigmoid(-split_heads(bwd_raw, HK))
    log_fwd = jnp.log1p(-key_fwd) + log_decay[0].T[:, :, None]
    log_bwd = jnp.log1p(-key_bwd) + log_decay[1].T[:, :, None]
    out_fwd, decay_fwd, ending_fwd, read_fwd = local_direction(queries, key_fwd, values, log_fwd)
    out_back, decay_bwd, ending_bwd, read_bwd = local_direction(
        jnp.flip(queries, 1), jnp.flip(key_bwd, 1), jnp.flip(values, 1), jnp.flip(log_bwd, 1)
    )
    positions = (lax.axis_index(SP) * length + jnp.arange(length, dtype=jnp.int32)).astype(
        jnp.float32
    )
    att_queries = (
        rotate(att_query_raw.astype(jnp.float32).reshape(length, -1, 2, AK), positions)
        * AK ** (-0.5)
    ).astype(jnp.bfloat16)
    att_keys = (
        rotate(att_key_raw.astype(jnp.float32).reshape(length, -1, 2, AK), positions)
        .astype(jnp.bfloat16)
        .reshape(length, -1)
    )
    att_heads = att_queries.shape[1]
    initial = (
        jnp.full((att_heads, 2, length), -jnp.inf, jnp.float32),
        jnp.zeros((att_heads, 2, length), jnp.float32),
        jnp.zeros((att_heads, 2, length, AV), jnp.float32),
    )
    identity = (jnp.ones_like(decay_fwd), jnp.zeros_like(ending_fwd))
    entry_fwd = entering((decay_fwd, ending_fwd), SP, link, identity, False)[1]
    entry_bwd = entering((decay_bwd, ending_bwd), SP, link, identity, True)[1]
    piece = in_one_piece((att_keys, att_value_raw), SP, 0, 1)
    running = attend(initial, att_queries, piece[0], piece[1])
    out_fwd = out_fwd + jnp.einsum("hld,hdv->hlv", read_fwd, entry_fwd)
    out_back = out_back + jnp.einsum("hld,hdv->hlv", read_bwd, entry_bwd)
    rec_rows = rms_scale(out_fwd + jnp.flip(out_back, 1), rec_gain)
    rec_rows = rec_rows.transpose(1, 0, 2).reshape(length, -1).astype(jnp.bfloat16)
    peak_values, totals, summed = running
    ratio = summed / totals[..., None]
    mixed_heads = ratio[:, 0] - lambdas[:, None, None] * ratio[:, 1]
    att_rows = (
        rms_scale(mixed_heads, att_gain).transpose(1, 0, 2).reshape(length, -1).astype(jnp.bfloat16)
    )
    rec_all, att_all = (
        lax.all_to_all(rec_rows, "tp", split_axis=0, concat_axis=1, tiled=True),
        lax.all_to_all(att_rows, "tp", split_axis=0, concat_axis=1, tiled=True),
    )
    projected_out = jnp.dot(rec_all, out_rec, preferred_element_type=jnp.float32) + jnp.dot(
        att_all, out_att, preferred_element_type=jnp.float32
    )
    return projected_out.astype(jnp.bfloat16)


def solution(mesh):
    torus = Mesh(mesh.devices.reshape(8, 4, mesh.shape["tp"]), ("sp_0", "sp_1", "tp"))
    in_specs = (
        P(SP_TP, None),
        P(),
        P(None, "tp"),
        P(None, "tp"),
        P(None, "tp"),
        P(None, "tp"),
        P(None, "tp"),
        P(None, SP, "tp"),
        P(),
        P(None, "tp"),
        P(None, "tp"),
        P(None, "tp"),
        P("tp"),
        P(),
        P(),
        P(),
    )
    out_specs = P(SP_TP, None)
    return jax.shard_map(
        on_device, mesh=torus, in_specs=in_specs, out_specs=out_specs, check_vma=False
    )
```

profile of v0, /device:TPU:1, one launch (start us, length us, event | category | flops | bytes accessed | tf_op | source)
XLA Modules:
  0.0 368.9 jit_solution(11481244566510974270)
XLA Ops:
  10.4 6.8 %all-to-all-start = ((bf16[8,64,2048]{2,1,0:T(8,128)(2,1)}), bf16[8,64,2048]{2,1,0:T(8,128)(2,1)S(1)}, u32[]{:S(2)}, u32[]{:S(2)}) async-start(bf16[8,64,2048]{2,1,0:T(8,128)(2,1)} %broadcast_in_dim.32), calls=%async_computation | async-start | bytes 4194304 | tf_op jit(solution)/shard_map/all_to_all | solution.py:30
  26.1 17.4 %all-to-all-done = bf16[8,64,2048]{2,1,0:T(8,128)(2,1)S(1)} async-done(((bf16[8,64,2048]{2,1,0:T(8,128)(2,1)}), bf16[8,64,2048]{2,1,0:T(8,128)(2,1)S(1)}, u32[]{:S(2)}, u32[]{:S(2)}) %all-to-all-start) | async-done | bytes 2097184 | tf_op jit(solution)/shard_map/all_to_all | solution.py:30
  43.5 4.4 %convolution_convert_fusion = bf16[512,896]{1,0:T(8,128)(2,1)S(1)} fusion(bf16[512,2048]{1,0:T(8,128)(2,1)S(1)} %bitcast.374, bf16[2048,896]{1,0:T(8,128)(2,1)} %constant_dynamic-update-slice_fusion), kind=kOutput, calls=%fused_computation.34 | convolution fusion | flops 1879506944 | bytes 6684672 | tf_op jit(solution)/shard_map/dot_general | solution.py:208
  57.0 6.2 %while.42 = (s32[]{:T(128)}, f32[1,128,128]{2,1,0:T(8,128)S(1)}, bf16[8,1,128,128]{3,2,1,0:T(8,128)(2,1)S(1)}, f32[8,1,128]{2,1,0:T(1,128)}, f32[8,1,128,128]{3,2,1,0:T(8,128)S(1)}, /*index=5*/s32[]{:T(128)}, s32[]{:T(128)}) while((s32[]{:T(128)}, f32[1,128,128]{2,1,0:T(8,128)S(1)}, bf16[8,1,128,128]{3,2,1,0:T(8,128)(2,1)S(1)}, ...), condition=%wide.region_8.9_spmd.clone, body=%wide.region_7.8_spmd.clone.sunk | while | flops 65539 | bytes 296556 | solution.py:124
  63.3 9.9 %all-gather.6 = bf16[4,129,128]{2,1,0:T(8,128)(2,1)S(1)} all-gather(bf16[1,129,128]{2,1,0:T(8,128)(2,1)S(1)} %maximum_bitcast_fusion.2), channel_id=4, replica_groups=mesh['sp_0'=8,'sp_1'=4,'tp'=8] {'sp_1'}, dimensions={0}, use_global_device_ids=true | all-gather | bytes 165120 | tf_op jit(solution)/shard_map/all_gather | solution.py:51
  73.3 23.6 %all-gather.7 = bf16[8,129,128]{2,1,0:T(8,128)(2,1)S(1)} all-gather(bf16[1,129,128]{2,1,0:T(8,128)(2,1)S(1)} %maximum_bitcast_fusion.3), channel_id=5, replica_groups=mesh['sp_0'=8,'sp_1'=4,'tp'=8] {'sp_0'}, dimensions={0}, use_global_device_ids=true | all-gather | bytes 297216 | tf_op jit(solution)/shard_map/all_gather | solution.py:51
  100.5 6.2 %while.41 = (s32[]{:T(128)}, f32[1,128,128]{2,1,0:T(8,128)S(1)}, bf16[8,1,128,128]{3,2,1,0:T(8,128)(2,1)S(1)}, f32[8,1,128]{2,1,0:T(1,128)}, f32[8,1,128,128]{3,2,1,0:T(8,128)S(1)}, /*index=5*/s32[]{:T(128)}, s32[]{:T(128)}) while((s32[]{:T(128)}, f32[1,128,128]{2,1,0:T(8,128)S(1)}, bf16[8,1,128,128]{3,2,1,0:T(8,128)(2,1)S(1)}, ...), condition=%wide.region_3.4_spmd.clone, body=%wide.region_2.3_spmd.clone.sunk | while | flops 65539 | bytes 296556 | solution.py:124
  106.8 11.3 %all-gather.4 = bf16[4,129,128]{2,1,0:T(8,128)(2,1)S(1)} all-gather(bf16[1,129,128]{2,1,0:T(8,128)(2,1)S(1)} %maximum_bitcast_fusion), channel_id=2, replica_groups=mesh['sp_0'=8,'sp_1'=4,'tp'=8] {'sp_1'}, dimensions={0}, use_global_device_ids=true | all-gather | bytes 165120 | tf_op jit(solution)/shard_map/all_gather | solution.py:51
  118.3 22.5 %all-gather.5 = bf16[8,129,128]{2,1,0:T(8,128)(2,1)S(1)} all-gather(bf16[1,129,128]{2,1,0:T(8,128)(2,1)S(1)} %maximum_bitcast_fusion.1), channel_id=3, replica_groups=mesh['sp_0'=8,'sp_1'=4,'tp'=8] {'sp_0'}, dimensions={0}, use_global_device_ids=true | all-gather | bytes 297216 | tf_op jit(solution)/shard_map/all_gather | solution.py:51
  142.8 16.7 %all-to-all-start.1 = ((bf16[8,64,128]{2,1,0:T(8,128)(2,1)}), bf16[8,64,128]{2,1,0:T(8,128)(2,1)S(1)}, u32[]{:S(2)}, u32[]{:S(2)}) async-start(bf16[8,64,128]{2,1,0:T(8,128)(2,1)} %bitcast.75), calls=%async_computation.1 | async-start | bytes 262144 | tf_op jit(solution)/shard_map/all_to_all | solution.py:267
  159.5 5.7 %fusion.265 = (bf16[16384,128]{1,0:T(8,128)(2,1)}, bf16[16384,128]{1,0:T(8,128)(2,1)}) fusion(bf16[16384,256]{1,0:T(8,128)(2,1)} %all-gather.10.cloned.1.call-done), kind=kLoop, calls=%fused_computation.394 | loop fusion | bytes 16777216 | tf_op jit(solution)/shard_map/split | solution.py:88
  165.2 14.7 %reshape.1565 = bf16[16,1024,1,2,64]{4,3,1,0,2:T(2,128)(2,1)} reshape(bf16[16384,128]{1,0:T(8,128)(2,1)} %get-tuple-element.274) | data formatting | bytes 8388608 | tf_op jit(solution)/shard_map/reshape | solution.py:162
  180.0 20.1 %copy.138 = bf16[16,1024,1,2,64]{1,4,3,2,0:T(8,128)(2,1)} copy(bf16[16,1024,1,2,64]{4,3,1,0,2:T(2,128)(2,1)} %reshape.1565) | data formatting | bytes 8388608
  200.1 146.9 %while.43 = (s32[]{:T(128)}, f32[1,2,512]{2,1,0:T(2,128)S(1)}, f32[1,2,512]{2,1,0:T(2,128)S(1)}, f32[1,2,512,128]{3,2,1,0:T(8,128)S(1)}, bf16[16,1024,1,2,64]{1,...) while((s32[]{:T(128)}, f32[1,2,512]{2,1,0:T(2,128)S(1)}, ...), condition=%wide.region_15.16_spmd.clone, body=%wide.region_12.15_spmd.clone.sunk | while | flops 408295424 | bytes 31129748 | solution.py:183
  200.1 3.7 bitcast_reduce_fusion.2
  203.7 2.9 fusion.291
  209.3 3.7 bitcast_reduce_fusion.2
  212.9 2.9 fusion.291
  218.4 3.7 bitcast_reduce_fusion.2
  222.1 2.9 fusion.291
  227.6 3.7 bitcast_reduce_fusion.2
  231.3 2.9 fusion.291
  236.8 3.7 bitcast_reduce_fusion.2
  240.5 2.9 fusion.291
  246.0 3.7 bitcast_reduce_fusion.2
  249.7 2.9 fusion.291
  255.2 3.7 bitcast_reduce_fusion.2
  258.8 2.9 fusion.291
  264.3 3.7 bitcast_reduce_fusion.2
  268.0 2.9 fusion.291
  273.5 3.7 bitcast_reduce_fusion.2
  277.2 2.9 fusion.291
  282.7 3.7 bitcast_reduce_fusion.2
  286.4 2.9 fusion.291
  291.9 3.7 bitcast_reduce_fusion.2
  295.6 2.9 fusion.291
  301.1 3.7 bitcast_reduce_fusion.2
  304.8 2.9 fusion.291
  310.3 3.7 bitcast_reduce_fusion.2
  319.4 3.7 bitcast_reduce_fusion.2
  323.1 2.9 fusion.291
  328.6 3.7 bitcast_reduce_fusion.2
  332.3 2.9 fusion.291
  337.8 3.7 bitcast_reduce_fusion.2
  341.5 2.9 fusion.291
  348.2 4.8 %all-to-all-start.2 = ((bf16[8,64,128]{2,1,0:T(8,128)(2,1)}), bf16[8,64,128]{2,1,0:T(8,128)(2,1)S(1)}, u32[]{:S(2)}, u32[]{:S(2)}) async-start(bf16[8,64,128]{2,1,0:T(8,128)(2,1)} %multiply_convert_fusion), calls=%async_computation.2 | async-start | bytes 262144 | tf_op jit(solution)/shard_map/all_to_all | solution.py:268
  353.1 3.0 fusion.73
  358.3 3.7 %fusion.23 = bf16[64,2048]{1,0:T(8,128)(2,1)} fusion(f32[64,2048]{1,0:T(8,128)S(1)} %fusion.73, bf16[1024,2048]{1,0:T(8,128)(2,1)} %param.37, bf16[8,64,128]{2,1,0:T(8,128)(2,1)S(1)} %all-to-all-done.2), kind=kOutput, calls=%fused_computation.33 | convolution fusion | flops 268697600 | bytes 5111808 | tf_op jit(solution)/shard_map/dot_general | solution.py:270
  (259 shorter events, 86.0 us)
Async XLA Ops:
  6.5 10.8 %copy-start.8 = (f32[2,512,1]{1,2,0:T(1,128)S(1)}, f32[2,512,1]{1,2,0:T(1,128)}, u32[]{:S(2)}) copy-start(f32[2,512,1]{1,2,0:T(1,128)} %param.29) | copy-start | bytes 12292
  7.7 10.1 %copy-start.9 = (f32[2,128]{1,0:T(2,128)S(1)}, f32[2,128]{1,0:T(2,128)}, u32[]{:S(2)}) copy-start(f32[2,128]{1,0:T(2,128)} %param.28) | copy-start | bytes 3076
  7.7 10.1 %copy-start.2 = (bf16[2048,128]{1,0:T(8,128)(2,1)S(1)}, bf16[2048,128]{1,0:T(8,128)(2,1)}, u32[]{:S(2)}) copy-start(bf16[2048,128]{1,0:T(8,128)(2,1)} %param.24) | copy-start | bytes 1572868
  10.4 8.3 %copy-start.3 = (bf16[2048,128]{1,0:T(8,128)(2,1)S(1)}, bf16[2048,128]{1,0:T(8,128)(2,1)}, u32[]{:S(2)}) copy-start(bf16[2048,128]{1,0:T(8,128)(2,1)} %param.25) | copy-start | bytes 1572868
  10.4 33.1 %all-to-all-start = ((bf16[8,64,2048]{2,1,0:T(8,128)(2,1)}), bf16[8,64,2048]{2,1,0:T(8,128)(2,1)S(1)}, u32[]{:S(2)}, u32[]{:S(2)}) async-start(bf16[8,64,2048]{2,1,0:T(8,128)(2,1)} %broadcast_in_dim.32), calls=%async_computation | async-start | bytes 4194304 | tf_op jit(solution)/shard_map/all_to_all | solution.py:30
  17.3 142.3 %all-gather.10.cloned.1.call-start = ((), (), s32[]{:S(2)}) async-start(), calls=%async_computation.3 | async-start | bytes 8650752 | tf_op jit(solution)/shard_map/all_gather | solution.py:88
  17.4 6.0 %copy-start.4 = (bf16[2048,128]{1,0:T(8,128)(2,1)S(1)}, bf16[2048,128]{1,0:T(8,128)(2,1)}, u32[]{:S(2)}) copy-start(bf16[2048,128]{1,0:T(8,128)(2,1)} %param.31) | copy-start | bytes 1572868
  17.4 7.0 %copy-start.5 = (bf16[2048,128]{1,0:T(8,128)(2,1)S(1)}, bf16[2048,128]{1,0:T(8,128)(2,1)}, u32[]{:S(2)}) copy-start(bf16[2048,128]{1,0:T(8,128)(2,1)} %param.32) | copy-start | bytes 1572868
  17.4 7.8 %copy-start.6 = (bf16[2048,128]{1,0:T(8,128)(2,1)S(1)}, bf16[2048,128]{1,0:T(8,128)(2,1)}, u32[]{:S(2)}) copy-start(bf16[2048,128]{1,0:T(8,128)(2,1)} %param.33) | copy-start | bytes 1572868
  47.9 0.9 copy-start.1
  57.0 43.4 %copy-start.12 = (f32[128]{0:T(128)S(1)}, f32[128]{0:T(128)}, u32[]{:S(2)}) copy-start(f32[128]{0:T(128)} %get-tuple-element.352) | copy-start | bytes 1540
  97.0 0.7 copy-start.7
  100.2 41.8 %copy-start.10 = (f32[128]{0:T(128)S(1)}, f32[128]{0:T(128)}, u32[]{:S(2)}) copy-start(f32[128]{0:T(128)} %param.30) | copy-start | bytes 1540
  142.8 205.4 %all-to-all-start.1 = ((bf16[8,64,128]{2,1,0:T(8,128)(2,1)}), bf16[8,64,128]{2,1,0:T(8,128)(2,1)S(1)}, u32[]{:S(2)}, u32[]{:S(2)}) async-start(bf16[8,64,128]{2,1,0:T(8,128)(2,1)} %bitcast.75), calls=%async_computation.1 | async-start | bytes 262144 | tf_op jit(solution)/shard_map/all_to_all | solution.py:267
  200.1 147.4 %copy-start.11 = (f32[128]{0:T(128)S(1)}, f32[128]{0:T(128)}, u32[]{:S(2)}) copy-start(f32[128]{0:T(128)} %param.35) | copy-start | bytes 1540
  203.7 3.4 copy-start
  212.9 3.4 copy-start
  222.1 3.4 copy-start
  231.3 3.4 copy-start
  240.5 3.4 copy-start
  249.6 3.4 copy-start
  258.8 3.4 copy-start
  268.0 3.4 copy-start
  277.2 3.4 copy-start
  286.4 3.4 copy-start
  295.6 3.4 copy-start
  304.7 3.4 copy-start
  313.9 3.4 copy-start
  323.1 3.4 copy-start
  332.3 3.4 copy-start
  341.5 3.4 copy-start
  348.2 10.1 %all-to-all-start.2 = ((bf16[8,64,128]{2,1,0:T(8,128)(2,1)}), bf16[8,64,128]{2,1,0:T(8,128)(2,1)S(1)}, u32[]{:S(2)}, u32[]{:S(2)}) async-start(bf16[8,64,128]{2,1,0:T(8,128)(2,1)} %multiply_convert_fusion), calls=%async_computation.2 | async-start | bytes 262144 | tf_op jit(solution)/shard_map/all_to_all | solution.py:268
Sparse Core Ops, SparseCore 0:
  53.2 101.1 all-gather.9
where the time goes:
time: 372 us; the launch traced here: 369 us
  matrix products  106 us (28%)
  local copies, waits for them, and re-layouts  70.9 us (19%)
  blocking collectives  67.4 us (18%)
  other arithmetic  60.9 us (16%)
  starting transfers between devices  28.3 us (8%)
  waiting for transfers between devices  19.6 us (5%)
  between operations  14.7 us (4%)
    all_gather x4, blocking collectives, all_in_one(): both, at, found = (lax.all_gather(jnp.concatenate(lines), axis), 0, {})  67.4 us
    dot_general x16, matrix products, absorb(): jnp.einsum('qhmd,khmd->hmqk', queries, key_block, preferred_element_type=...  58.6 us
    reduce_sum x16, other arithmetic, absorb(): totals = totals * shrink + jnp.sum(weights_raw, axis=-1)  46.8 us
    dot_general x16, matrix products, absorb(): jnp.einsum('hmqk,khv->hmqv', weights_raw.astype(jnp.bfloat16), value_bloc...  32.8 us
    unnamed x31, local copies, waits for them, and re-layouts  28.8 us
    all_to_all x1, waiting for transfers between devices, copy_for_each(): return lax.all_to_all(copies, axis, split_axis=0, concat_axis=0, tiled=True)  17.4 us
    all_to_all x1, starting transfers between devices, on_device(): lax.all_to_all(rec_rows, 'tp', split_axis=0, concat_axis=1, tiled=True)  16.7 us
    reshape x1, local copies, waits for them, and re-layouts, attend(): key_rows.reshape(row_count // span_rows, span_rows, head_count, 2, AK)  14.7 us
  transfers between devices with their start and end apart: 4, of which 2 were waited for; matrix products, arithmetic and copies ran while one was open for 58% of the time, Pallas kernels for 0%

commit v1 on v0

v1 whole, which is shorter than its diff:
```python
import math

import jax
import jax.numpy as jnp
import numpy as np
from jax import lax
from jax.experimental import pallas as pl
from jax.experimental.pallas import tpu as pltpu
from jax.sharding import Mesh
from jax.sharding import PartitionSpec as P

HK = 128
AK = 64
BLOCK = 64
SP = ("sp_0", "sp_1")
SP_TP = ("sp_0", "sp_1", "tp")
NZ, NX, NY = 8, 4, 4
ROWS = 64
LEN = 512
D = 2048
NCOL = 896
EPS = 1e-06
THETA = 500000.0
LOG2E = 1.4426950408889634
F32 = jnp.float32
BF16 = jnp.bfloat16
MESH = pl.DeviceIdType.MESH
VMEM_SPEC = pl.BlockSpec(memory_space=pltpu.VMEM)
ANY_SPEC = pl.BlockSpec(memory_space=pl.ANY)
VMEM_LIMIT = 60 * 1024 * 1024


def remote(src, dst, send_sem, recv_sem, device):
    return pltpu.make_async_remote_copy(
        src_ref=src,
        dst_ref=dst,
        send_sem=send_sem,
        recv_sem=recv_sem,
        device_id=device,
        device_id_type=MESH,
    )


def meet(devices):
    barrier = pltpu.get_barrier_semaphore()
    for device in devices:
        pl.semaphore_signal(barrier, inc=1, device_id=device, device_id_type=MESH)
    pl.semaphore_wait(barrier, len(devices))


def dot(a, b):
    return jnp.dot(a, b, preferred_element_type=F32)


def dot_nt(a, b):
    return lax.dot_general(a, b, (((1,), (1,)), ((), ())), preferred_element_type=F32)


def project_kernel(
    tok_ref, gain_ref, cos_a, sin_a, cos_b, sin_b, *refs
):
    weights = refs[:7]
    qt_ref, kv_ref, rec_ref = refs[7:10]
    xbuf, wbuf, attbuf, wsem, send, recv = refs[10:]
    t = lax.axis_index("tp")
    y, c = t // 2, t % 2
    right = lax.rem(y + 1, NY) * 2 + c
    left = lax.rem(y + NY - 1, NY) * 2 + c
    far = lax.rem(y + 2, NY) * 2 + c
    partner = 2 * y + 1 - c

    loads = [
        pltpu.make_async_copy(w, wbuf.at[:, pl.ds(128 * k, 128)], wsem.at[k])
        for k, w in enumerate(weights)
    ]
    for load in loads:
        load.start()
    meet([{"tp": right}, {"tp": left}, {"tp": partner}])

    half = ROWS // 2
    part = (pl.ds(0, half), pl.ds(half, half))
    own = [tok_ref.at[p] for p in part]

    def to(src, slot, k, number, device):
        return remote(src, xbuf.at[slot, part[k]], send.at[number], recv.at[number], {"tp": device})

    copies = {}

    def launch(src, slot, k, number, device):
        copies[number] = to(src, slot, k, number, device)
        copies[number].start()

    launch(own[0], t, 0, 0, right)
    launch(own[1], t, 1, 3, left)
    launch(own[1], t, 1, 1, right)
    launch(own[0], t, 0, 2, left)
    launch(own[0], t, 0, 4, partner)
    launch(own[1], t, 1, 5, partner)

    def arrived(slot, k, number):
        to(own[k], slot, k, number, right).wait_recv()

    xbuf[t] = tok_ref[...]
    for load in loads:
        load.wait()

    z, x = lax.axis_index("sp_0"), lax.axis_index("sp_1")
    block = z * NX + x
    cb = cos_b[pl.ds(block, 1), :]
    sb = sin_b[pl.ds(block, 1), :]
    lane = lax.broadcasted_iota(jnp.int32, (1, 128), 1)
    low = lax.rem(lane, 64) < 32

    def turned(v, cosine, sine):
        other = jnp.where(low, pltpu.roll(v, 96, 1), pltpu.roll(v, 32, 1))
        return v * cosine + other * sine

    def process(yy):
        pair = xbuf[pl.ds(2 * yy, 2)].reshape(2 * ROWS, D).astype(F32)
        scale = lax.rsqrt(jnp.mean(pair * pair, axis=1, keepdims=True) + EPS)
        normed = (pair * scale * gain_ref[...]).astype(BF16)
        out = dot(normed, wbuf[...])
        rows = pl.ds(pl.multiple_of(yy * 128, 128), 128)
        rec_ref[rows, :] = out[:, :512].astype(BF16)
        ca, sa = cos_a[rows, :], sin_a[rows, :]
        cosine = ca * cb - sa * sb
        sine = sa * cb + ca * sb
        signed = jnp.where(low, -sine, sine)
        raw = out[:, 512:].astype(BF16).astype(F32)
        attbuf[0, rows, :] = turned(raw[:, 0:128], cosine, signed) * (AK**-0.5 * LOG2E)
        attbuf[1, rows, :] = turned(raw[:, 128:256], cosine, signed)
        attbuf[2, rows, :] = raw[:, 256:384]

    slot_l, slot_r = left, right
    arrived(partner, 0, 4)
    arrived(partner, 1, 5)
    process(y)

    arrived(slot_l, 0, 0)
    launch(xbuf.at[slot_l, part[0]], slot_l, 0, 6, right)
    launch(xbuf.at[slot_l, part[0]], slot_l, 0, 8, partner)
    arrived(slot_r, 1, 3)
    launch(xbuf.at[slot_r, part[1]], slot_r, 1, 7, left)
    launch(xbuf.at[slot_r, part[1]], slot_r, 1, 9, partner)
    arrived(slot_l, 1, 1)
    launch(xbuf.at[slot_l, part[1]], slot_l, 1, 10, partner)
    arrived(slot_r, 0, 2)
    launch(xbuf.at[slot_r, part[0]], slot_r, 0, 11, partner)
    mate_l, mate_r, mate_far = left + 1 - 2 * c, right + 1 - 2 * c, far + 1 - 2 * c
    arrived(mate_l, 0, 8)
    arrived(mate_l, 1, 10)
    process(left // 2)
    arrived(mate_r, 1, 9)
    arrived(mate_r, 0, 11)
    process(right // 2)
    arrived(far, 0, 6)
    launch(xbuf.at[far, part[0]], far, 0, 12, partner)
    arrived(far, 1, 7)
    launch(xbuf.at[far, part[1]], far, 1, 13, partner)
    arrived(mate_far, 0, 12)
    arrived(mate_far, 1, 13)
    process(far // 2)

    qt_ref[...] = attbuf[0].T.astype(BF16)
    value_t = attbuf[2].T.astype(BF16)
    for s in range(2):
        kv_ref[s, 0:256, :] = attbuf[1, 256 * s : 256 * (s + 1), :].astype(BF16)
        kv_ref[s, 256:384, :] = value_t[:, 256 * s : 256 * s + 128]
        kv_ref[s, 384:512, :] = value_t[:, 256 * s + 128 : 256 * s + 256]
    for number in range(14):
        copies[number].wait_send()


def rotary_tables():
    i = np.arange(AK // 2, dtype=np.float64)
    freq = THETA ** (-(i * 2.0 / AK))
    freq = np.tile(freq, 4)[None, :]
    within = np.arange(LEN, dtype=np.float64)[:, None] * freq
    starts = np.arange(NZ * NX, dtype=np.float64)[:, None] * LEN * freq
    return [
        jnp.asarray(f(v).astype(np.float32)) for v in (within, starts) for f in (np.cos, np.sin)
    ]


def project(tokens, norm_gain, weights):
    cos_a, sin_a, cos_b, sin_b = rotary_tables()
    return pl.pallas_call(
        project_kernel,
        out_shape=(
            jax.ShapeDtypeStruct((128, LEN), BF16),
            jax.ShapeDtypeStruct((2, 512, 128), BF16),
            jax.ShapeDtypeStruct((LEN, 512), BF16),
        ),
        in_specs=[VMEM_SPEC] * 6 + [ANY_SPEC] * 7,
        out_specs=(VMEM_SPEC,) * 3,
        scratch_shapes=[
            pltpu.VMEM((8, ROWS, D), BF16),
            pltpu.VMEM((D, NCOL), BF16),
            pltpu.VMEM((3, LEN, 128), F32),
            pltpu.SemaphoreType.DMA((7,)),
            pltpu.SemaphoreType.DMA((14,)),
            pltpu.SemaphoreType.DMA((14,)),
        ],
        compiler_params=pltpu.CompilerParams(
            collective_id=0, has_side_effects=True, vmem_limit_bytes=VMEM_LIMIT
        ),
        name="gather_project",
    )(tokens, norm_gain.reshape(1, D), cos_a, sin_a, cos_b, sin_b, *weights)


def exact_cumulative(triangle, logs):
    first = logs.astype(BF16)
    rest = logs - first.astype(F32)
    second = rest.astype(BF16)
    third = (rest - second.astype(F32)).astype(BF16)
    return dot(triangle, first) + dot(triangle, second) + dot(triangle, third)


def recurrence_kernel(rec_ref, leak_ref, decay_ref, out_ref, read_ref, state_ref):
    blocks = LEN // BLOCK
    raw_q = rec_ref[:, 0:128].astype(F32)
    rq = raw_q / (1.0 + jnp.exp(-raw_q))
    value = rec_ref[:, 384:512]
    value_t = value.astype(F32).T.astype(BF16)
    row = lax.broadcasted_iota(jnp.int32, (256, 256), 0)
    col = lax.broadcasted_iota(jnp.int32, (256, 256), 1)
    same = (row // BLOCK) == (col // BLOCK)
    upper = lax.broadcasted_iota(jnp.int32, (128, 1), 0) < BLOCK
    total_out = None
    for side in range(2):
        raw = rec_ref[:, 128 * (side + 1) : 128 * (side + 2)].astype(F32)
        key = leak_ref[side : side + 1, :] / (1.0 + jnp.exp(raw))
        logs = jnp.log1p(-key) + decay_ref[side]
        mask = same & ((row >= col) if side == 0 else (row <= col))
        triangle = mask.astype(F32).astype(BF16)
        cum = jnp.concatenate(
            [exact_cumulative(triangle, logs[256 * h : 256 * (h + 1)]) for h in range(2)], axis=0
        )
        cum3 = cum.reshape(blocks, BLOCK, 128)
        at_mid, at_last = (BLOCK // 2 - 1, BLOCK - 1) if side == 0 else (BLOCK // 2, 0)
        middle = cum3[:, at_mid : at_mid + 1, :]
        last = cum3[:, at_last : at_last + 1, :]
        key3, rq3 = key.reshape(cum3.shape), rq.reshape(cum3.shape)
        qs = (rq3 * jnp.exp(cum3 - middle)).reshape(LEN, 128).astype(BF16)
        ks = (key3 * jnp.exp(middle - cum3)).reshape(LEN, 128).astype(BF16)
        kl = (key3 * jnp.exp(last - cum3)).reshape(LEN, 128)
        qc = (rq3 * jnp.exp(cum3)).reshape(LEN, 128).astype(BF16)
        within = []
        for h in range(2):
            part = slice(256 * h, 256 * (h + 1))
            scores = jnp.where(mask, dot_nt(qs[part], ks[part]), 0.0).astype(BF16)
            within.append(dot(scores, value[part]))
        order = range(blocks) if side == 0 else reversed(range(blocks))
        state = jnp.zeros((128, 128), F32)
        carried, before = [None] * blocks, [None] * blocks
        running = jnp.zeros((1, 128), F32)
        for b in order:
            carried[b] = dot_nt(qc[BLOCK * b : BLOCK * (b + 1)], state.astype(BF16))
            pair = b // 2
            keys = kl[128 * pair : 128 * (pair + 1)]
            keys = jnp.where(upper if b % 2 == 0 else ~upper, keys, 0.0).astype(BF16)
            added = dot(value_t[:, 128 * pair : 128 * (pair + 1)], keys)
            before[b] = running
            running = running + last[b]
            state = state * jnp.exp(last[b]) + added
        out = jnp.concatenate(within, axis=0) + jnp.concatenate(carried, axis=0)
        total_out = out if total_out is None else total_out + out
        reach = (cum3 + jnp.stack(before, axis=0)).reshape(LEN, 128)
        read_ref[side] = (rq * jnp.exp(reach)).astype(BF16)
        state_ref[side, 0:128, :] = state.astype(BF16)
        state_ref[side, 128:144, :] = jnp.broadcast_to(jnp.exp(running), (16, 128)).astype(BF16)
    out_ref[...] = total_out


def recurrence(rec, gate_leak, log_decay):
    return pl.pallas_call(
        recurrence_kernel,
        out_shape=(
            jax.ShapeDtypeStruct((LEN, 128), F32),
            jax.ShapeDtypeStruct((2, LEN, 128), BF16),
            jax.ShapeDtypeStruct((2, 144, 128), BF16),
        ),
        in_specs=[VMEM_SPEC] * 3,
        out_specs=(VMEM_SPEC,) * 3,
        compiler_params=pltpu.CompilerParams(vmem_limit_bytes=VMEM_LIMIT),
        name="local_recurrence",
    )(rec, gate_leak, log_decay)


def mix_kernel(
    qt_ref, kv_ref, recout_ref, read_ref, state_ref, lam_ref, attgain_ref, recgain_ref,
    mixed_ref,
    kvbuf, qbuf, qz, acc, peak, sendo, recvo, sendm, recvm, stbuf, totals, inside, chain_in, chain_out,
    r_send, r_recv, l_send, l_recv, q_send, q_recv, o_send, o_recv, m_send, m_recv, s_send, s_recv,
    c_send, c_recv,
):
    z, x = lax.axis_index("sp_0"), lax.axis_index("sp_1")
    up = {"sp_0": lax.rem(z + 1, NZ)}
    down = {"sp_0": lax.rem(z + NZ - 1, NZ)}
    beside = [None] + [{"sp_1": lax.rem(x + p, NX)} for p in range(1, NX)]
    meet([up, down] + beside[1:])

    ring = {}

    def rightward(step, s):
        src = kv_ref.at[s] if step == 0 else kvbuf.at[NZ - step, s]
        return remote(
            src, kvbuf.at[NZ - 1 - step, s], r_send.at[step, s], r_recv.at[step, s], up
        )

    def leftward(step, s):
        src = kv_ref.at[s] if step == 0 else kvbuf.at[step, s]
        return remote(src, kvbuf.at[step + 1, s], l_send.at[step, s], l_recv.at[step, s], down)

    def start_right(step, s):
        ring["r", step, s] = rightward(step, s)
        ring["r", step, s].start()

    def start_left(step, s):
        ring["l", step, s] = leftward(step, s)
        ring["l", step, s].start()

    q_copies = [
        remote(qt_ref, qbuf.at[NX - p], q_send.at[p], q_recv.at[NX - p], beside[p])
        for p in range(1, NX)
    ]
    s_copies = [
        remote(state_ref, stbuf.at[NX - p], s_send.at[p], s_recv.at[NX - p], beside[p])
        for p in range(1, NX)
    ]
    for copy in q_copies:
        copy.start()
    for s in range(2):
        start_right(0, s)
        start_left(0, s)
    for copy in s_copies:
        copy.start()

    kvbuf[0] = kv_ref[...]
    stbuf[0] = state_ref[...]
    upper = lax.broadcasted_iota(jnp.int32, (128, 1), 0) < AK

    def spread(p, source):
        for h in range(2):
            piece = source[:, 256 * h : 256 * (h + 1)].astype(F32)
            qz[p, h] = jnp.where(upper, piece, 0.0).astype(BF16)
            qz[p, 2 + h] = jnp.where(upper, 0.0, piece).astype(BF16)

    ones = jnp.ones((16, 256), BF16)

    def flash(p, slots, first):
        def tile(k, carry):
            query = qz[p, k]
            scores = [
                dot(kvbuf[r, s, 0:256, :], query) for r in slots for s in range(2)
            ]
            top = None
            for piece in scores:
                here = jnp.max(piece, axis=0, keepdims=True)
                top = here if top is None else jnp.maximum(top, here)
            if not first:
                old = peak[p, k, 0:1, :]
                top = jnp.maximum(top, old)
            weights = [jnp.exp2(piece - top).astype(BF16) for piece in scores]
            summed = None
            n = 0
            for r in slots:
                for s in range(2):
                    values = jnp.concatenate(
                        [kvbuf[r, s, 256:384, :], kvbuf[r, s, 384:512, :]], axis=1
                    )
                    values = jnp.concatenate([values, ones], axis=0)
                    term = dot(values, weights[n])
                    summed = term if summed is None else summed + term
                    n += 1
            if first:
                acc[p, k] = summed
            else:
                acc[p, k] = acc[p, k] * jnp.exp2(old - top) + summed
            peak[p, k] = jnp.broadcast_to(top, (8, 256))
            return carry

        lax.fori_loop(0, 4, tile, 0)

    spread(0, qt_ref[...])
    flash(0, (0,), True)
    for p in range(1, NX):
        q_copies[NX - p - 1].wait_recv()
        spread(p, qbuf[p])

    def forward(step):
        for s in range(2):
            rightward(step - 1, s).wait_recv()
            if step < 3 or s == 0:
                start_right(step, s)
            leftward(step - 1, s).wait_recv()
            if step < 3 or s == 1:
                start_left(step, s)

    forward(1)
    for p in range(1, NX):
        s_copies[NX - p - 1].wait_recv()

    for side in range(2):
        order = range(NX) if side == 0 else reversed(range(NX))
        total_s, total_d = jnp.zeros((128, 128), F32), jnp.ones((1, 128), F32)
        inside_s, inside_d = total_s, total_d
        for k in order:
            rel = lax.rem(k - x + NX, NX)
            piece_s = stbuf[rel, side, 0:128, :].astype(F32)
            piece_d = stbuf[rel, side, 128:144, :].astype(F32)[0:1, :]
            total_s = total_s * piece_d + piece_s
            total_d = total_d * piece_d
            passed = (k < x) if side == 0 else (k > x)
            inside_s = jnp.where(passed, total_s, inside_s)
            inside_d = jnp.where(passed, total_d, inside_d)
        totals[side, 0:128, :] = total_s
        totals[side, 128:136, :] = jnp.broadcast_to(total_d, (8, 128))
        inside[side, 0:128, :] = inside_s
        inside[side, 128:136, :] = jnp.broadcast_to(inside_d, (8, 128))

    @pl.when(z == 0)
    def _():
        chain_in[0] = jnp.zeros((128, 128), F32)

    @pl.when(z == NZ - 1)
    def _():
        chain_in[1] = jnp.zeros((128, 128), F32)

    def chain_copy(side):
        return remote(
            chain_out.at[side], chain_in.at[side], c_send.at[side], c_recv.at[side],
            up if side == 0 else down,
        )

    def chain(hop):
        for side in range(2):
            turn = (z == hop) if side == 0 else (z == NZ - 1 - hop)

            @pl.when(turn)
            def _():
                if hop > 0:
                    chain_copy(side).wait_recv()
                if hop < NZ - 1:
                    chain_out[side] = (
                        chain_in[side] * totals[side, 128:129, :] + totals[side, 0:128, :]
                    )
                    chain_copy(side).start()

    chain(0)
    for p in range(1, NX):
        flash(p, (0, 7, 1), True)
        chain(p)
    flash(0, (7, 1), False)
    forward(2)
    chain(4)
    for p in range(NX):
        flash(p, (6, 2), False)
        if p < 3:
            chain(5 + p)
    forward(3)
    rightward(3, 0).wait_recv()
    leftward(3, 1).wait_recv()

    o_copies = {}
    for p in (2, 1, 3):
        flash(p, (5, 3, 4), False)
        for k in range(4):
            inverse = 1.0 / acc[p, k, 128:129, :]
            sendo[p, k] = (acc[p, k, 0:128, :] * inverse).astype(BF16)
            sendm[p, k, 0:8, :] = peak[p, k]
            sendm[p, k, 8:16, :] = acc[p, k, 128:136, :]
        o_copies[p] = (
            remote(sendo.at[p], recvo.at[NX - p], o_send.at[p], o_recv.at[NX - p], beside[p]),
            remote(sendm.at[p], recvm.at[NX - p], m_send.at[p], m_recv.at[NX - p], beside[p]),
        )
        for copy in o_copies[p]:
            copy.start()
    flash(0, (5, 3, 4), False)

    out = recout_ref[...]
    for side in range(2):
        entry = chain_in[side] * inside[side, 128:129, :] + inside[side, 0:128, :]
        out = out + dot_nt(read_ref[side], entry.astype(BF16))
    out = out * lax.rsqrt(jnp.mean(out * out, axis=1, keepdims=True) + EPS) * recgain_ref[...]
    mixed_ref[:, 0:128] = out.astype(BF16)

    for p in (2, 3, 1):
        for copy in o_copies[NX - p]:
            copy.wait_recv()
    lam = lam_ref[0:1, 0:1]
    for h in range(2):
        maps = []
        for m in range(2):
            k = 2 * m + h
            tops = [peak[0, k, 0:1, :]] + [recvm[p, k, 0:1, :] for p in range(1, NX)]
            sums = [acc[0, k, 128:129, :]] + [recvm[p, k, 8:9, :] for p in range(1, NX)]
            top = tops[0]
            for other in tops[1:]:
                top = jnp.maximum(top, other)
            shares = [a * jnp.exp2(b - top) for a, b in zip(sums, tops)]
            whole = shares[0] + shares[1] + shares[2] + shares[3]
            inverse = 1.0 / whole
            value = acc[0, k, 0:128, :] * (jnp.exp2(tops[0] - top) * inverse)
            for p in range(1, NX):
                value = value + recvo[p, k].astype(F32) * (shares[p] * inverse)
            maps.append(value)
        mixed = maps[0] - lam * maps[1]
        mixed = mixed * lax.rsqrt(jnp.mean(mixed * mixed, axis=0, keepdims=True) + EPS)
        mixed = mixed * attgain_ref[...]
        mixed_ref[256 * h : 256 * (h + 1), 128:256] = mixed.T.astype(BF16)

    for copy in ring.values():
        copy.wait_send()
    for copy in q_copies + s_copies:
        copy.wait_send()
    for pair in o_copies.values():
        for copy in pair:
            copy.wait_send()

    @pl.when(z < NZ - 1)
    def _():
        chain_copy(0).wait_send()

    @pl.when(z > 0)
    def _():
        chain_copy(1).wait_send()


def mix(qt, kv, recout, read, state, lambdas, att_gain, rec_gain):
    dma = pltpu.SemaphoreType.DMA
    return pl.pallas_call(
        mix_kernel,
        out_shape=jax.ShapeDtypeStruct((LEN, 256), BF16),
        in_specs=[VMEM_SPEC] * 8,
        out_specs=VMEM_SPEC,
        scratch_shapes=[
            pltpu.VMEM((NZ, 2, 512, 128), BF16),
            pltpu.VMEM((NX, 128, LEN), BF16),
            pltpu.VMEM((NX, 4, 128, 256), BF16),
            pltpu.VMEM((NX, 4, 144, 256), F32),
            pltpu.VMEM((NX, 4, 8, 256), F32),
            pltpu.VMEM((NX, 4, 128, 256), BF16),
            pltpu.VMEM((NX, 4, 128, 256), BF16),
            pltpu.VMEM((NX, 4, 16, 256), F32),
            pltpu.VMEM((NX, 4, 16, 256), F32),
            pltpu.VMEM((NX, 2, 144, 128), BF16),
            pltpu.VMEM((2, 136, 128), F32),
            pltpu.VMEM((2, 136, 128), F32),
            pltpu.VMEM((2, 128, 128), F32),
            pltpu.VMEM((2, 128, 128), F32),
            dma((4, 2)), dma((4, 2)), dma((4, 2)), dma((4, 2)),
            dma((NX,)), dma((NX,)), dma((NX,)), dma((NX,)), dma((NX,)), dma((NX,)),
            dma((NX,)), dma((NX,)), dma((2,)), dma((2,)),
        ],
        compiler_params=pltpu.CompilerParams(
            collective_id=1, has_side_effects=True, vmem_limit_bytes=VMEM_LIMIT
        ),
        name="attend_and_link",
    )(
        qt, kv, recout, read, state, lambdas.reshape(1, 1), att_gain.reshape(128, 1),
        rec_gain.reshape(1, 128),
    )


def output_kernel(mixed_ref, wrec_ref, watt_ref, out_ref, got, wr, wa, wsem, send, recv):
    t = lax.axis_index("tp")
    loads = [
        pltpu.make_async_copy(wrec_ref, wr, wsem.at[0]),
        pltpu.make_async_copy(watt_ref, wa, wsem.at[1]),
    ]
    for load in loads:
        load.start()
    others = [lax.rem(t + k, 8) for k in range(1, 8)]
    meet([{"tp": o} for o in others])
    copies = []
    for k, o in enumerate(others):
        rows = pl.ds(pl.multiple_of(o * ROWS, ROWS), ROWS)
        copies.append(
            remote(mixed_ref.at[rows, :], got.at[7 - k], send.at[k], recv.at[7 - k], {"tp": o})
        )
        copies[-1].start()
    mine = pl.ds(pl.multiple_of(t * ROWS, ROWS), ROWS)
    got[0] = mixed_ref[mine, :]
    for load in loads:
        load.wait()
    total = None
    for k in range(8):
        if k > 0:
            remote(
                mixed_ref.at[mine, :], got.at[k], send.at[0], recv.at[k], {"tp": others[0]}
            ).wait_recv()
        source = lax.rem(t + k, 8)
        rows = pl.ds(pl.multiple_of(source * 128, 128), 128)
        term = dot(got[k, :, 0:128], wr[rows, :]) + dot(got[k, :, 128:256], wa[rows, :])
        total = term if total is None else total + term
    out_ref[...] = total.astype(BF16)
    for copy in copies:
        copy.wait_send()


def output(mixed, out_rec, out_att):
    dma = pltpu.SemaphoreType.DMA
    return pl.pallas_call(
        output_kernel,
        out_shape=jax.ShapeDtypeStruct((ROWS, D), BF16),
        in_specs=[VMEM_SPEC, ANY_SPEC, ANY_SPEC],
        out_specs=VMEM_SPEC,
        scratch_shapes=[
            pltpu.VMEM((8, ROWS, 256), BF16),
            pltpu.VMEM((1024, D), BF16),
            pltpu.VMEM((1024, D), BF16),
            dma((2,)), dma((8,)), dma((8,)),
        ],
        compiler_params=pltpu.CompilerParams(
            collective_id=2, has_side_effects=True, vmem_limit_bytes=VMEM_LIMIT
        ),
        name="exchange_output",
    )(mixed, out_rec, out_att)


def on_device(
    tokens, norm_gain, rec_query, fwd_gate, bwd_gate, rec_value, gate_leak, log_decay, rec_gain,
    att_query, att_key, att_value, lambdas, att_gain, out_rec, out_att,
):
    weights = (rec_query, fwd_gate, bwd_gate, rec_value, att_query, att_key, att_value)
    qt, kv, rec = project(tokens, norm_gain, weights)
    recout, read, state = recurrence(rec, gate_leak, log_decay)
    mixed = mix(qt, kv, recout, read, state, lambdas, att_gain, rec_gain)
    return output(mixed, out_rec, out_att)


def solution(mesh):
    torus = Mesh(mesh.devices.reshape(NZ, NX, mesh.shape["tp"]), SP_TP)
    tp = P(None, "tp")
    in_specs = (
        P(SP_TP, None), P(), tp, tp, tp, tp, tp, P(None, SP, "tp"), P(), tp, tp, tp, P("tp"), P(),
        P(), P(),
    )
    return jax.shard_map(
        on_device, mesh=torus, in_specs=in_specs, out_specs=P(SP_TP, None), check_vma=False
    )
```

time: 372 us -> 114 us (0.31)
  Pallas kernels: 0 us -> 110 us
  matrix products: 106 us -> 0 us
  local copies, waits for them, and re-layouts: 70.9 us -> 3.43 us
  blocking collectives: 67.4 us -> 0 us
  other arithmetic: 60.9 us -> 0 us
  starting transfers between devices: 28.3 us -> 0 us
  waiting for transfers between devices: 19.6 us -> 0 us
  between operations: 14.7 us -> 0.7 us
    pallas_call x0 -> x4, Pallas kernels: none -> 110 us  [the longest x1 73.1 us: mix(): pl.pallas_call(mix_kernel, out_shape=jax.ShapeDtypeStruct((LEN, 256), BF1...]
    dot_general x43 -> x0, matrix products: 106 us -> none  [the longest x16 58.6 us: absorb(): jnp.einsum('qhmd,khmd->hmqk', queries, key_block, preferred_element_type=...]
    all_gather x4 -> x0, blocking collectives: 67.4 us -> none  [all_in_one(): both, at, found = (lax.all_gather(jnp.concatenate(lines), axis), 0, {})]
    reduce_sum x19 -> x0, other arithmetic: 49.3 us -> none  [the longest x16 46.8 us: absorb(): totals = totals * shrink + jnp.sum(weights_raw, axis=-1)]
    all_to_all x3 -> x0, starting transfers between devices: 28.3 us -> none  [the longest x1 16.7 us: on_device(): lax.all_to_all(rec_rows, 'tp', split_axis=0, concat_axis=1, tiled=True)]
    unnamed x31 -> x6, local copies, waits for them, and re-layouts: 28.8 us -> 2.69 us
    all_to_all x3 -> x0, waiting for transfers between devices: 19.6 us -> none  [the longest x1 17.4 us: copy_for_each(): return lax.all_to_all(copies, axis, split_axis=0, concat_axis=0, tiled=True)]
    reshape x3 -> x1, local copies, waits for them, and re-layouts: 15 us -> 0.74 us  [mix(): att_gain.reshape(128, 1)]
  transfers between devices with their start and end apart: 4 -> 0, of which waited for: 2 -> 0; matrix products, arithmetic and copies ran while one was open for 58% -> 0% of each run, Pallas kernels for 0% -> 0%
where the time goes in v1:
time: 114 us
  Pallas kernels  110 us (96%)
  local copies, waits for them, and re-layouts  3.43 us (3%)
    pallas_call x1, Pallas kernels, mix(): pl.pallas_call(mix_kernel, out_shape=jax.ShapeDtypeStruct((LEN, 256), BF1...  73.1 us
    pallas_call x1, Pallas kernels, project(): pl.pallas_call(project_kernel, out_shape=(jax.ShapeDtypeStruct((128, LEN)...  19.3 us
    pallas_call x1, Pallas kernels, output(): pl.pallas_call(output_kernel, out_shape=jax.ShapeDtypeStruct((ROWS, D), B...  12.9 us
    pallas_call x1, Pallas kernels, recurrence(): pl.pallas_call(recurrence_kernel, out_shape=(jax.ShapeDtypeStruct((LEN, 1...  4.71 us
    unnamed x6, local copies, waits for them, and re-layouts  2.69 us

profile of v1, /device:TPU:1, one launch (start us, length us, event | category | flops | bytes accessed | tf_op | source)
XLA Modules:
  0.0 114.1 jit_solution(15890871629826646266)
XLA Ops:
  0.0 0.0 copy-start
  0.0 0.0 copy-start.1
  0.0 19.3 %gather_project.1 = (bf16[128,512]{1,0:T(8,128)(2,1)}, bf16[2,512,128]{2,1,0:T(8,128)(2,1)}, bf16[512,512]{1,0:T(8,128)(2,1)}) custom-call(bf16[64,2048]{1,0:T(8,128)(2,1)} %tok_ref.1, f32[1,2048]{1,0:T(1,128)} %bitcast.5, f32[512,128]{1,0:T(8,128)} %constant.8.clone.cos_a, f32[512,128]{1,0:T(8,128)} %constant.9.clone.sin_a, ...), custom_call_target="tpu_custom_call" | custom-call | tf_op jit(solution)/shard_map/gather_project/pallas_call | solution.py:187
  19.3 0.0 copy-done
  19.3 1.0 copy.21.decay_ref
  20.4 4.7 %local_recurrence.1 = (f32[512,128]{1,0:T(8,128)}, bf16[2,512,128]{2,1,0:T(8,128)(2,1)}, bf16[2,144,128]{2,1,0:T(8,128)(2,1)}) custom-call(bf16[512,512]{1,0:T(8,128)(2,1)} %get-tuple-element.13.rec_ref, f32[2,128]{1,0:T(2,128)} %leak_ref.1, f32[2,512,1]{2,1,0:T(8,128)} %copy.21.decay_ref), custom_call_target="tpu_custom_call" | custom-call | tf_op jit(solution)/shard_map/local_recurrence/pallas_call | solution.py:276
  25.7 0.0 copy-done.1
  25.7 0.7 copy.22.attgain_ref
  26.5 73.1 %attend_and_link.1.mixed_ref = bf16[512,256]{1,0:T(8,128)(2,1)} custom-call(bf16[128,512]{1,0:T(8,128)(2,1)} %get-tuple-element.11.qt_ref, bf16[2,512,128]{2,1,0:T(8,128)(2,1)} %get-tuple-element.12.kv_ref, f32[512,128]{1,0:T(8,128)} %get-tuple-element.14.recout_ref, bf16[2,512,128]{2,1,0:T(8,128)(2,1)} %get-tuple-element.15.read_ref, ...), custom_call_target="tpu_custom_call" | custom-call | tf_op jit(solution)/shard_map/attend_and_link/pallas_call | solution.py:532
  99.5 12.9 %exchange_output.1 = bf16[64,2048]{1,0:T(8,128)(2,1)} custom-call(bf16[512,256]{1,0:T(8,128)(2,1)} %attend_and_link.1.mixed_ref, bf16[1024,2048]{1,0:T(8,128)(2,1)} %wrec_ref.1, bf16[1024,2048]{1,0:T(8,128)(2,1)} %watt_ref.1), custom_call_target="tpu_custom_call" | custom-call | tf_op jit(solution)/shard_map/exchange_output/pallas_call | solution.py:604
  112.5 1.7 %copy.25 = bf16[64,2048]{1,0:T(8,128)(2,1)} copy(bf16[64,2048]{1,0:T(8,128)(2,1)} %exchange_output.1) | data formatting | bytes 524288
Async XLA Ops:
  0.0 19.3 %copy-start = (f32[2,512,1]{1,2,0:T(1,128)S(1)}, f32[2,512,1]{1,2,0:T(1,128)}, u32[]{:S(2)}) copy-start(f32[2,512,1]{1,2,0:T(1,128)} %param.27) | copy-start | bytes 12292
  0.0 25.7 %copy-start.1 = (f32[128]{0:T(128)S(1)}, f32[128]{0:T(128)}, u32[]{:S(2)}) copy-start(f32[128]{0:T(128)} %param.33) | copy-start | bytes 1540
